TPU v7x, 32 devices: a whole 2x2x4 slice. The times are simulated.
32 devices in a mesh: grp: 2 (over y), fs: 4 (over z), tp: 4 (over x, core).
Axes of the slice: x: 2, y: 2, z: 4, core: 2. Of those that a mesh axis runs over, the one named last changes fastest.
Arguments:
- tokens: bfloat16 [4096, 2048], P(('grp', 'fs'), 'tp'), parts along dimension 0, may hold values from -36 to 36
- query_matrix: bfloat16 [2048, 1024], P('fs', 'tp'), may hold values from -0.125 to 0.125
- key_weight: bfloat16 [2048, 1024], P('fs', 'tp'), may hold values from -0.125 to 0.125
- value_weight: bfloat16 [2048, 2048], P('fs', 'tp'), may hold values from -0.125 to 0.125
- forget_lower_factor: bfloat16 [2048, 32], replicated, may hold values from -0.125 to 0.125
- decay_up: bfloat16 [32, 1024], replicated, may hold values from -1 to 1
- decay_bias: float32 [1024], replicated, may hold values from -1 to 8
- log_extra: float32 [4096, 1024], P(('grp', 'fs'), 'tp'), parts along dimension 0, may hold values from -0.7 to 0
- head_gain: float32 [256], replicated, may hold values from 0.1 to 1.9
- out_weight: bfloat16 [2048, 2048], P('tp', 'fs'), may hold values from -0.125 to 0.125
- mix_gain: float32 [2048], P('tp'), may hold values from 0.1 to 1.9
- up_weight: bfloat16 [2048, 8192], P('fs', 'tp'), may hold values from -0.125 to 0.125
- down_weight: bfloat16 [8192, 2048], P('tp', 'fs'), may hold values from -0.0625 to 0.0625
- out_gain: float32 [2048], P('tp'), may hold values from 0.1 to 1.9
Outputs:
- layer_out: bfloat16 [4096, 2048], P(('grp', 'fs'), 'tp'), parts along dimension 0
There are 2 independent parts, one for each index of `grp`. A program takes and returns all parts, laid end to end along the dimension named above; an argument that names none is the same for every part. Nothing has to cross between parts.
All inputs are finite; a program needn't handle non-finite values.
Results may differ from a plain program's by a relative error of at most 0.015.
Values may be sent and summed in bfloat16 or wider, within the bound.
A program may use at most 64 MiB of HBM per device.

v0:
```python
import jax
import jax.numpy as jnp
from jax import lax
from jax.sharding import PartitionSpec as P

D = 2048
DK = 128
DV = 256
SEGMENT_LENGTH = 64
ALPHA = 2.0**0.5
TAU = 16.0
EPS = 1e-05
HIGH = lax.Precision.HIGHEST


def block_scan(queries, key_rows, value_rows, log_decay):
    span = queries.shape[2]
    causal = (jnp.arange(span)[:, None] >= jnp.arange(span)[None, :])[:, :, None]

    def step(state, inputs):
        query_block, key_block, value_block, decay_block = inputs
        cumul = jnp.cumsum(decay_block, axis=1)
        last_cum = cumul[:, -1:, :]
        carried = jnp.einsum("hcd,hde->hce", query_block * jnp.exp(cumul), state, precision=HIGH)
        differ = cumul[:, :, None, :] - cumul[:, None, :, :]
        weights = jnp.exp(jnp.where(causal, differ, -jnp.inf))
        scores = jnp.sum(query_block[:, :, None, :] * key_block[:, None, :, :] * weights, axis=-1)
        within = jnp.einsum("hij,hje->hie", scores, value_block, precision=HIGH)
        fresh = jnp.einsum(
            "hcd,hce->hde", key_block * jnp.exp(last_cum - cumul), value_block, precision=HIGH
        )
        new_state = jnp.exp(last_cum[:, 0, :])[:, :, None] * state + fresh
        return (new_state, carried + within)

    start = jnp.zeros((queries.shape[1], queries.shape[3], value_rows.shape[3]), jnp.float32)
    _, outputs = lax.scan(step, start, (queries, key_rows, value_rows, log_decay))
    return outputs


def layer_norm(summed, gain_cols):
    row_total, row_squares = lax.psum(
        (jnp.sum(summed, axis=1), jnp.sum(summed * summed, axis=1)), "tp"
    )
    row_mean = row_total / D
    row_var = row_squares / D - row_mean * row_mean
    centered = summed - row_mean[:, None]
    return (centered * lax.rsqrt(row_var[:, None] + EPS) * gain_cols).astype(jnp.bfloat16)


def local(
    tokens,
    query_matrix,
    key_weight,
    value_weight,
    forget_lower_factor,
    decay_up,
    decay_bias,
    log_extra,
    head_gain,
    out_weight,
    mix_gain,
    up_weight,
    down_weight,
    out_gain,
):
    gathered = lax.all_gather(tokens, "tp", axis=1, tiled=True)
    row_count = gathered.shape[0]
    key_cols = query_matrix.shape[1]
    value_cols = value_weight.shape[1]
    local_heads = key_cols // DK
    block_pieces = (
        lax.all_gather(query_matrix, "fs", axis=0, tiled=True),
        lax.all_gather(key_weight, "fs", axis=0, tiled=True),
        lax.all_gather(value_weight, "fs", axis=0, tiled=True),
    )
    columns = gathered
    queries, key_rows, value_rows = tuple(
        (
            jnp.dot(columns, shard_piece, preferred_element_type=jnp.float32)
            for shard_piece in block_pieces
        )
    )
    queries = queries.astype(jnp.bfloat16)
    key_rows = key_rows.astype(jnp.bfloat16)
    value_rows = value_rows.astype(jnp.bfloat16)
    low = jnp.dot(gathered, forget_lower_factor, preferred_element_type=jnp.float32).astype(
        jnp.bfloat16
    )
    offset_cols = lax.axis_index("tp") * key_cols
    local_up = lax.dynamic_slice_in_dim(decay_up, offset_cols, key_cols, 1)
    local_bias = lax.dynamic_slice_in_dim(decay_bias, offset_cols, key_cols, 0)
    gate_pre = jnp.dot(low, local_up, preferred_element_type=jnp.float32) + local_bias
    log_decay = jax.nn.log_sigmoid(gate_pre) / TAU + log_extra
    count = row_count // SEGMENT_LENGTH

    def blocks(array, depth):
        return (
            array.astype(jnp.float32)
            .reshape(count, SEGMENT_LENGTH, local_heads, depth)
            .transpose(0, 2, 1, 3)
        )

    attended = block_scan(
        blocks(queries, DK) * DK ** (-0.5),
        blocks(key_rows, DK),
        blocks(value_rows, DV),
        blocks(log_decay, DK),
    )
    attended = attended.transpose(0, 2, 1, 3).reshape(row_count, local_heads, DV)
    scaled = (
        attended
        * lax.rsqrt(jnp.mean(attended * attended, axis=-1, keepdims=True) + EPS)
        * head_gain
    )
    mixed_heads = scaled.reshape(row_count, value_cols).astype(jnp.bfloat16)
    mix_terms = jnp.dot(
        mixed_heads,
        lax.all_gather(out_weight, "fs", axis=1, tiled=True),
        preferred_element_type=jnp.float32,
    )
    mix = lax.psum_scatter(
        mix_terms.astype(jnp.bfloat16), "tp", scatter_dimension=1, tiled=True
    ).astype(jnp.float32)
    normed_local = layer_norm(ALPHA * tokens.astype(jnp.float32) + mix, mix_gain)
    normed_rows = lax.all_gather(normed_local, "tp", axis=1, tiled=True)
    columns = normed_rows
    hidden = jnp.dot(
        columns,
        lax.all_gather(up_weight, "fs", axis=0, tiled=True),
        preferred_element_type=jnp.float32,
    )
    activation = jnp.square(jax.nn.relu(hidden)).astype(jnp.bfloat16)
    down_terms = jnp.dot(
        activation,
        lax.all_gather(down_weight, "fs", axis=1, tiled=True),
        preferred_element_type=jnp.float32,
    )
    down = lax.psum_scatter(
        down_terms.astype(jnp.bfloat16), "tp", scatter_dimension=1, tiled=True
    ).astype(jnp.float32)
    return layer_norm(ALPHA * normed_local.astype(jnp.float32) + down, out_gain)


def solution(mesh):
    in_specs = (
        P(("grp", "fs"), "tp"),
        P("fs", "tp"),
        P("fs", "tp"),
        P("fs", "tp"),
        P(),
        P(),
        P(),
        P(("grp", "fs"), "tp"),
        P(),
        P("tp", "fs"),
        P("tp"),
        P("fs", "tp"),
        P("tp", "fs"),
        P("tp"),
    )
    out_specs = P(("grp", "fs"), "tp")
    return jax.shard_map(local, mesh=mesh, in_specs=in_specs, out_specs=out_specs, check_vma=False)
```

profile of v0, /device:TPU:0, one launch (start us, length us, event | category | flops | bytes accessed | tf_op | source)
XLA Modules:
  0.0 615.8 jit_solution(9214274555413043903)
XLA Ops:
  10.8 23.4 %all-gather.9.cloned.1.call-done = bf16[512,2048]{1,0:T(8,128)(2,1)} async-done(((bf16[512,512]{1,0:T(8,128)(2,1)}), bf16[512,2048]{1,0:T(8,128)(2,1)}) %all-gather.9.cloned.1.call-update) | async-done | bytes 2097168 | tf_op jit(solution)/shard_map/all_gather | solution.py:66
  34.2 2.8 fusion.31
  38.1 25.7 %all-gather.15.cloned.1.call-done = bf16[2048,256]{1,0:T(8,128)(2,1)} async-done(((bf16[512,256]{1,0:T(8,128)(2,1)}), bf16[2048,256]{1,0:T(8,128)(2,1)}) %all-gather.15.cloned.1.call-update) | async-done | bytes 1048592 | tf_op jit(solution)/shard_map/all_gather | solution.py:72
  63.8 2.6 fusion.26
  67.4 25.3 %all-gather.11.cloned.1.call-done = bf16[2048,256]{1,0:T(8,128)(2,1)} async-done(((bf16[512,256]{1,0:T(8,128)(2,1)}), bf16[2048,256]{1,0:T(8,128)(2,1)}) %all-gather.11.cloned.1.call-update) | async-done | bytes 1048592 | tf_op jit(solution)/shard_map/all_gather | solution.py:73
  92.8 2.6 fusion.24
  96.4 42.9 %all-gather.13.cloned.1.call-done = bf16[2048,512]{1,0:T(8,128)(2,1)} async-done(((bf16[512,512]{1,0:T(8,128)(2,1)}), bf16[2048,512]{1,0:T(8,128)(2,1)}) %all-gather.13.cloned.1.call-update) | async-done | bytes 2097168 | tf_op jit(solution)/shard_map/all_gather | solution.py:74
  139.3 3.5 fusion.22
  145.6 38.5 %while.13 = (s32[]{:T(128)}, f32[2,128,256]{2,1,0:T(8,128)S(1)}, f32[8,2,64,256]{3,2,1,0:T(8,128)S(1)}, f32[8,2,64,128]{3,2,1,0:T(8,128)}, f32[8,2,64,128]{3,2,1...) while((s32[]{:T(128)}, f32[2,128,256]{2,1,0:T(8,128)S(1)}, ...), condition=%wide.region_3.4_spmd.clone, body=%wide.region_0.3_spmd.clone.sunk | while | flops 132444160 | bytes 2539644 | solution.py:36
  147.4 1.9 multiply_reduce_fusion.5
  152.2 1.9 multiply_reduce_fusion.5
  157.0 1.9 multiply_reduce_fusion.5
  161.8 1.9 multiply_reduce_fusion.5
  186.1 4.2 convolution_convert_fusion.1
  190.4 30.1 %reduce-scatter.3.cloned.1.call-done = bf16[512,512]{1,0:T(8,128)(2,1)} async-done(((bf16[512,2048]{1,0:T(8,128)(2,1)}), bf16[512,512]{1,0:T(8,128)(2,1)}) %reduce-scatter.3.cloned.1.call-update) | async-done | bytes 524304 | tf_op jit(solution)/shard_map/reduce_scatter | solution.py:121
  221.8 5.8 all-reduce.1
  227.6 2.1 multiply_convert_fusion.2
  231.4 21.6 %all-gather.19.cloned.1.call-done = bf16[512,2048]{1,0:T(8,128)(2,1)} async-done(((bf16[512,512]{1,0:T(8,128)(2,1)}), bf16[512,2048]{1,0:T(8,128)(2,1)}) %all-gather.19.cloned.1.call-update) | async-done | bytes 2097168 | tf_op jit(solution)/shard_map/all_gather | solution.py:125
  253.1 151.2 %all-gather.21.cloned.1.call-done = bf16[2048,2048]{1,0:T(8,128)(2,1)} async-done(((bf16[512,2048]{1,0:T(8,128)(2,1)}), bf16[2048,2048]{1,0:T(8,128)(2,1)}) %all-gather.21.cloned.1.call-update) | async-done | bytes 8388624 | tf_op jit(solution)/shard_map/all_gather | solution.py:129
  404.3 149.4 %all-gather.23.cloned.1.call-done = bf16[2048,2048]{1,0:T(8,128)(2,1)} async-done(((bf16[2048,512]{1,0:T(8,128)(2,1)}), bf16[2048,2048]{1,0:T(8,128)(2,1)}) %all-gather.23.cloned.1.call-update) | async-done | bytes 8388624 | tf_op jit(solution)/shard_map/all_gather | solution.py:135
  553.7 16.5 %convolution_convert_fusion = bf16[512,2048]{1,0:T(8,128)(2,1)} fusion(bf16[2048,2048]{1,0:T(8,128)(2,1)} %all-gather.23.cloned.1.call-done, bf16[512,2048]{1,0:T(8,128)(2,1)} %all-gather.19.cloned.1.call-done, bf16[2048,2048]{1,0:T(8,128)(2,1)} %all-gather.21.cloned.1.call-done), kind=kOutput, calls=%fused_computation.29 | convolution fusion | flops 8594128896 | bytes 20971520 | tf_op jit(solution)/shard_map/dot_general | solution.py:133
  570.2 29.5 %reduce-scatter.5.cloned.1.call-done = bf16[512,512]{1,0:T(8,128)(2,1)} async-done(((bf16[512,2048]{1,0:T(8,128)(2,1)}), bf16[512,512]{1,0:T(8,128)(2,1)}) %reduce-scatter.5.cloned.1.call-update) | async-done | bytes 524304 | tf_op jit(solution)/shard_map/reduce_scatter | solution.py:138
  601.1 5.8 all-reduce
  606.9 2.1 multiply_convert_fusion.1
  (138 shorter events, 46.9 us)
Async XLA Ops:
  6.5 27.7 %copy-start = (bf16[2048,32]{0,1:T(8,128)(2,1)S(1)}, bf16[2048,32]{0,1:T(8,128)(2,1)}, u32[]{:S(2)}) copy-start(bf16[2048,32]{0,1:T(8,128)(2,1)} %param.20) | copy-start | bytes 393220
  6.5 3.4 copy-start.7
  6.5 27.7 %copy-start.8 = (f32[512,256]{1,0:T(8,128)S(1)}, f32[512,256]{1,0:T(8,128)}, u32[]{:S(2)}) copy-start(f32[512,256]{1,0:T(8,128)} %param.23) | copy-start | bytes 1572868
  6.5 27.7 %all-gather.9.cloned.1.call-start = ((), (), s32[]{:S(2)}) async-start(), calls=%async_computation.2 | async-start | bytes 2621440 | tf_op jit(solution)/shard_map/all_gather | solution.py:66
  7.3 56.5 %all-gather.15.cloned.1.call-start = ((), (), s32[]{:S(2)}) async-start(), calls=%async_computation.5 | async-start | bytes 1310720 | tf_op jit(solution)/shard_map/all_gather | solution.py:72
  8.0 84.8 %all-gather.11.cloned.1.call-start = ((), (), s32[]{:S(2)}) async-start(), calls=%async_computation.3 | async-start | bytes 1310720 | tf_op jit(solution)/shard_map/all_gather | solution.py:73
  8.7 130.5 %all-gather.13.cloned.1.call-start = ((), (), s32[]{:S(2)}) async-start(), calls=%async_computation.4 | async-start | bytes 2621440 | tf_op jit(solution)/shard_map/all_gather | solution.py:74
  9.3 176.8 %all-gather.17.cloned.1.call-start = ((), (), s32[]{:S(2)}) async-start(), calls=%async_computation.6 | async-start | bytes 2621440 | tf_op jit(solution)/shard_map/all_gather | solution.py:118
  9.9 210.5 %reduce-scatter.3.cloned.1.call-start = ((), (), s32[]{:S(2)}) async-start(), calls=%async_computation.7 | async-start | bytes 2621440 | tf_op jit(solution)/shard_map/reduce_scatter | solution.py:121
  143.4 1.0 copy-start.3
  143.4 1.2 copy-start.4
  190.3 30.1 %copy-start.2 = (bf16[512,512]{1,0:T(8,128)(2,1)S(1)}, bf16[512,512]{1,0:T(8,128)(2,1)}, u32[]{:S(2)}) copy-start(bf16[512,512]{1,0:T(8,128)(2,1)} %param.16) | copy-start | bytes 1572868
  190.3 37.3 %copy-start.5 = (f32[512]{0:T(512)S(1)}, f32[512]{0:T(512)}, u32[]{:S(2)}) copy-start(f32[512]{0:T(512)} %param.26) | copy-start | bytes 6148
  190.3 62.7 %all-gather.19.cloned.1.call-start = ((), (), s32[]{:S(2)}) async-start(), calls=%async_computation.8 | async-start | bytes 2621440 | tf_op jit(solution)/shard_map/all_gather | solution.py:125
  229.7 174.6 %all-gather.21.cloned.1.call-start = ((), (), s32[]{:S(2)}) async-start(), calls=%async_computation.9 | async-start | bytes 10485760 | tf_op jit(solution)/shard_map/all_gather | solution.py:129
  230.5 323.2 %all-gather.23.cloned.1.call-start = ((), (), s32[]{:S(2)}) async-start(), calls=%async_computation.10 | async-start | bytes 10485760 | tf_op jit(solution)/shard_map/all_gather | solution.py:135
  231.2 368.5 %reduce-scatter.5.cloned.1.call-start = ((), (), s32[]{:S(2)}) async-start(), calls=%async_computation.11 | async-start | bytes 2621440 | tf_op jit(solution)/shard_map/reduce_scatter | solution.py:138
  570.2 29.5 %copy-start.1 = (bf16[512,512]{1,0:T(8,128)(2,1)S(1)}, bf16[512,512]{1,0:T(8,128)(2,1)}, u32[]{:S(2)}) copy-start(bf16[512,512]{1,0:T(8,128)(2,1)} %multiply_convert_fusion.2) | copy-start | bytes 1572868
  570.2 36.7 %copy-start.6 = (f32[512]{0:T(512)S(1)}, f32[512]{0:T(512)}, u32[]{:S(2)}) copy-start(f32[512]{0:T(512)} %param.29) | copy-start | bytes 6148
Sparse Core Ops, SparseCore 0:
  8.9 25.2 all-gather.8
  35.8 27.9 all-gather.14
  65.4 27.3 all-gather.10
  94.2 45.0 all-gather.12
  140.7 44.4 all-gather.16
  190.4 29.9 reduce-scatter.2
  229.8 23.1 all-gather.18
  254.6 149.6 all-gather.20
  405.8 147.7 all-gather.22
  570.3 29.3 reduce-scatter.4
where the time goes:
time: 617 us; the launch traced here: 616 us
  waiting for transfers between devices  504 us (82%)
  matrix products  39.9 us (6%)
  other arithmetic  23.6 us (4%)
  local copies, waits for them, and re-layouts  22.3 us (4%)
  between operations  13.7 us (2%)
  blocking collectives  11.5 us (2%)
    all_gather x1, waiting for transfers between devices, local(): lax.all_gather(up_weight, 'fs', axis=0, tiled=True)  151 us
    all_gather x1, waiting for transfers between devices, local(): lax.all_gather(down_weight, 'fs', axis=1, tiled=True)  149 us
    all_gather x1, waiting for transfers between devices, local(): lax.all_gather(value_weight, 'fs', axis=0, tiled=True)  42.9 us
    reduce_scatter x1, waiting for transfers between devices, local(): lax.psum_scatter(mix_terms.astype(jnp.bfloat16), 'tp', scatter_dimension=...  30.1 us
    reduce_scatter x1, waiting for transfers between devices, local(): lax.psum_scatter(down_terms.astype(jnp.bfloat16), 'tp', scatter_dimension...  29.5 us
    all_gather x1, waiting for transfers between devices, local(): lax.all_gather(query_matrix, 'fs', axis=0, tiled=True)  25.7 us
    all_gather x1, waiting for transfers between devices, local(): lax.all_gather(key_weight, 'fs', axis=0, tiled=True)  25.3 us
    all_gather x1, waiting for transfers between devices, local(): gathered = lax.all_gather(tokens, 'tp', axis=1, tiled=True)  23.4 us
  transfers between devices with their start and end apart: 10, of which 9 were waited for; matrix products, arithmetic and copies ran while one was open for 9% of the time, Pallas kernels for 0%

commit v1 on v0

--- a/solution.py
+++ b/solution.py
@@ -11,6 +11,27 @@
 TAU = 16.0
 EPS = 1e-05
 HIGH = lax.Precision.HIGHEST
+
+
+def collect(x, axis, dim):
+    length, index, span = (lax.axis_size(axis), lax.axis_index(axis), x.shape[dim])
+    right = [(i, (i + 1) % length) for i in range(length)]
+    downward = [(i, (i - 1) % length) for i in range(length)]
+    whole = jnp.zeros((*x.shape[:dim], length * span, *x.shape[dim + 1 :]), x.dtype)
+    whole = lax.dynamic_update_slice_in_dim(whole, x, index * span, axis=dim)
+    from_left = from_right = x
+    half = length // 2
+    for step in range(1, half + 1):
+        from_left = lax.ppermute(from_left, axis, right)
+        whole = lax.dynamic_update_slice_in_dim(
+            whole, from_left, (index - step) % length * span, axis=dim
+        )
+        if step < length - half:
+            from_right = lax.ppermute(from_right, axis, downward)
+            whole = lax.dynamic_update_slice_in_dim(
+                whole, from_right, (index + step) % length * span, axis=dim
+            )
+    return whole
 
 
 def block_scan(queries, key_rows, value_rows, log_decay):
@@ -131,9 +152,7 @@
     )
     activation = jnp.square(jax.nn.relu(hidden)).astype(jnp.bfloat16)
     down_terms = jnp.dot(
-        activation,
-        lax.all_gather(down_weight, "fs", axis=1, tiled=True),
-        preferred_element_type=jnp.float32,
+        activation, collect(down_weight, "fs", 1), preferred_element_type=jnp.float32
     )
     down = lax.psum_scatter(
         down_terms.astype(jnp.bfloat16), "tp", scatter_dimension=1, tiled=True

time: 617 us -> 568 us (0.921)
  waiting for transfers between devices: 504 us -> 403 us
  starting transfers between devices: 0.53 us -> 37.1 us
  local copies, waits for them, and re-layouts: 22.3 us -> 37.5 us
    ppermute x0 -> x3, waiting for transfers between devices: none -> 192 us  [the longest x1 111 us: collect(): from_right = lax.ppermute(from_right, axis, downward)]
    all_gather x1 -> x0, waiting for transfers between devices: 149 us -> none  [local(): lax.all_gather(down_weight, 'fs', axis=1, tiled=True)]
    all_gather x1, waiting for transfers between devices: 151 us -> 29.9 us  [local(): lax.all_gather(up_weight, 'fs', axis=0, tiled=True)]
    ppermute x0 -> x3, starting transfers between devices: none -> 36.8 us  [the longest x2 34.7 us: collect(): from_left = lax.ppermute(from_left, axis, right)]
    all_gather x1, waiting for transfers between devices: 21.6 us -> 0.01 us  [local(): normed_rows = lax.all_gather(normed_local, 'tp', axis=1, tiled=True)]
    dynamic_update_slice x0 -> x4, local copies, waits for them, and re-layouts: none -> 10.9 us  [the longest x2 6.25 us: collect(): lax.dynamic_update_slice_in_dim(whole, from_left, (index - step) % length...]
  transfers between devices with their start and end apart: 10 -> 12, of which waited for: 9 -> 10; matrix products, arithmetic and copies ran while one was open for 9% -> 13% of each run, Pallas kernels for 0% -> 0%
where the time goes in v1:
time: 568 us; the launch traced here: 567 us
  waiting for transfers between devices  403 us (71%)
  matrix products  39.9 us (7%)
  local copies, waits for them, and re-layouts  37.5 us (7%)
  starting transfers between devices  37.1 us (7%)
  other arithmetic  23.8 us (4%)
  between operations  13.4 us (2%)
  blocking collectives  11.5 us (2%)
    ppermute x1, waiting for transfers between devices, collect(): from_right = lax.ppermute(from_right, axis, downward)  111 us
    ppermute x2, waiting for transfers between devices, collect(): from_left = lax.ppermute(from_left, axis, right)  81.7 us
    all_gather x1, waiting for transfers between devices, local(): lax.all_gather(value_weight, 'fs', axis=0, tiled=True)  42.8 us
    ppermute x2, starting transfers between devices, collect(): from_left = lax.ppermute(from_left, axis, right)  34.7 us
    reduce_scatter x1, waiting for transfers between devices, local(): lax.psum_scatter(mix_terms.astype(jnp.bfloat16), 'tp', scatter_dimension=...  30.1 us
    all_gather x1, waiting for transfers between devices, local(): lax.all_gather(up_weight, 'fs', axis=0, tiled=True)  29.9 us
    reduce_scatter x1, waiting for transfers between devices, local(): lax.psum_scatter(down_terms.astype(jnp.bfloat16), 'tp', scatter_dimension...  29.5 us
    all_gather x1, waiting for transfers between devices, local(): lax.all_gather(query_matrix, 'fs', axis=0, tiled=True)  25.7 us
  transfers between devices with their start and end apart: 12, of which 10 were waited for; matrix products, arithmetic and copies ran while one was open for 13% of the time, Pallas kernels for 0%

profile of v1, /device:TPU:0, one launch (start us, length us, event | category | flops | bytes accessed | tf_op | source)
XLA Modules:
  0.0 566.8 jit_solution(9671313118646140845)
XLA Ops:
  10.8 23.4 %all-gather.8.cloned.1.call-done = bf16[512,2048]{1,0:T(8,128)(2,1)} async-done(((bf16[512,512]{1,0:T(8,128)(2,1)}), bf16[512,2048]{1,0:T(8,128)(2,1)}) %all-gather.8.cloned.1.call-update) | async-done | bytes 2097168 | tf_op jit(solution)/shard_map/all_gather | solution.py:87
  34.2 2.8 fusion.31
  38.1 25.7 %all-gather.14.cloned.1.call-done = bf16[2048,256]{1,0:T(8,128)(2,1)} async-done(((bf16[512,256]{1,0:T(8,128)(2,1)}), bf16[2048,256]{1,0:T(8,128)(2,1)}) %all-gather.14.cloned.1.call-update) | async-done | bytes 1048592 | tf_op jit(solution)/shard_map/all_gather | solution.py:93
  63.8 2.6 fusion.26
  67.4 25.3 %all-gather.10.cloned.1.call-done = bf16[2048,256]{1,0:T(8,128)(2,1)} async-done(((bf16[512,256]{1,0:T(8,128)(2,1)}), bf16[2048,256]{1,0:T(8,128)(2,1)}) %all-gather.10.cloned.1.call-update) | async-done | bytes 1048592 | tf_op jit(solution)/shard_map/all_gather | solution.py:94
  92.8 2.6 fusion.24
  96.4 42.8 %all-gather.12.cloned.1.call-done = bf16[2048,512]{1,0:T(8,128)(2,1)} async-done(((bf16[512,512]{1,0:T(8,128)(2,1)}), bf16[2048,512]{1,0:T(8,128)(2,1)}) %all-gather.12.cloned.1.call-update) | async-done | bytes 2097168 | tf_op jit(solution)/shard_map/all_gather | solution.py:95
  139.3 3.5 fusion.22
  145.6 38.5 %while.13 = (s32[]{:T(128)}, f32[2,128,256]{2,1,0:T(8,128)S(1)}, f32[8,2,64,256]{3,2,1,0:T(8,128)S(1)}, f32[8,2,64,128]{3,2,1,0:T(8,128)}, f32[8,2,64,128]{3,2,1...) while((s32[]{:T(128)}, f32[2,128,256]{2,1,0:T(8,128)S(1)}, ...), condition=%wide.region_3.4_spmd.clone, body=%wide.region_0.3_spmd.clone.sunk | while | flops 132444160 | bytes 2540163 | solution.py:57
  186.1 4.2 convolution_convert_fusion.1
  190.4 30.1 %reduce-scatter.3.cloned.1.call-done = bf16[512,512]{1,0:T(8,128)(2,1)} async-done(((bf16[512,2048]{1,0:T(8,128)(2,1)}), bf16[512,512]{1,0:T(8,128)(2,1)}) %reduce-scatter.3.cloned.1.call-update) | async-done | bytes 524304 | tf_op jit(solution)/shard_map/reduce_scatter | solution.py:142
  221.8 5.8 %all-reduce.1 = (f32[512]{0:T(512)S(1)}, f32[512]{0:T(512)S(1)}) all-reduce(f32[512]{0:T(512)S(1)} %get-tuple-element.77, f32[512]{0:T(512)S(1)} %get-tuple-element.76), channel_id=1, replica_groups=mesh['grp'=2,'fs'=4,'tp'=4] {'tp'}, use_global_device_ids=true, to_apply=%region_9.10 | all-reduce | flops 1024 | bytes 8192 | tf_op jit(solution)/shard_map/psum | solution.py:62
  234.6 58.9 %collective-permute-done = bf16[2048,512]{1,0:T(8,128)(2,1)} collective-permute-done((bf16[2048,512]{1,0:T(8,128)(2,1)S(1)}, bf16[2048,512]{1,0:T(8,128)(2,1)}, u32[]{:S(2)}, u32[]{:S(2)}) %collective-permute-start) | collective-permute-done | bytes 2097184 | tf_op jit(solution)/shard_map/ppermute | solution.py:25
  293.4 32.9 %collective-permute-start.2 = (bf16[2048,512]{1,0:T(8,128)(2,1)}, bf16[2048,512]{1,0:T(8,128)(2,1)}, u32[]{:S(2)}, u32[]{:S(2)}) collective-permute-start(bf16[2048,512]{1,0:T(8,128)(2,1)} %collective-permute-done), channel_id=1, source_target_pairs={{0,4},{4,8},{8,12},{12,0},{1,5},{5,9},{9,13},{13,1},{2,6},{6,10},{... | collective-permute-start | bytes 6291464 | tf_op jit(solution)/shard_map/ppermute | solution.py:25
  326.4 4.3 broadcast_in_dim.29
  332.2 3.1 constant_dynamic-update-slice_fusion.2
  335.3 110.7 %collective-permute-done.1 = bf16[2048,512]{1,0:T(8,128)(2,1)} collective-permute-done((bf16[2048,512]{1,0:T(8,128)(2,1)S(1)}, bf16[2048,512]{1,0:T(8,128)(2,1)}, u32[]{:S(2)}, u32[]{:S(2)}) %collective-permute-start.1) | collective-permute-done | bytes 2097184 | tf_op jit(solution)/shard_map/ppermute | solution.py:30
  446.0 3.1 constant_dynamic-update-slice_fusion.1
  449.1 22.9 %collective-permute-done.2 = bf16[2048,512]{1,0:T(8,128)(2,1)} collective-permute-done((bf16[2048,512]{1,0:T(8,128)(2,1)}, bf16[2048,512]{1,0:T(8,128)(2,1)}, u32[]{:S(2)}, u32[]{:S(2)}) %collective-permute-start.2) | collective-permute-done | bytes 2097184 | tf_op jit(solution)/shard_map/ppermute | solution.py:25
  472.0 3.1 constant_dynamic-update-slice_fusion
  475.1 29.9 %all-gather.20.cloned.1.call-done = bf16[2048,2048]{1,0:T(8,128)(2,1)} async-done(((bf16[512,2048]{1,0:T(8,128)(2,1)}), bf16[2048,2048]{1,0:T(8,128)(2,1)}) %all-gather.20.cloned.1.call-update) | async-done | bytes 8388624 | tf_op jit(solution)/shard_map/all_gather | solution.py:150
  505.0 16.5 %convolution_convert_fusion = bf16[512,2048]{1,0:T(8,128)(2,1)} fusion(bf16[2048,2048]{1,0:T(8,128)(2,1)} %constant_dynamic-update-slice_fusion, bf16[512,2048]{1,0:T(8,128)(2,1)} %all-gather.18.cloned.1.call-done, bf16[2048,2048]{1,0:T(8,128)(2,1)} %all-gather.20.cloned.1.call-done), kind=kOutput, calls=%fused_computation.29 | convolution fusion | flops 8594128896 | bytes 20971520 | tf_op jit(solution)/shard_map/dot_general | solution.py:154
  521.5 29.5 %reduce-scatter.5.cloned.1.call-done = bf16[512,512]{1,0:T(8,128)(2,1)} async-done(((bf16[512,2048]{1,0:T(8,128)(2,1)}), bf16[512,512]{1,0:T(8,128)(2,1)}) %reduce-scatter.5.cloned.1.call-update) | async-done | bytes 524304 | tf_op jit(solution)/shard_map/reduce_scatter | solution.py:157
  552.3 5.8 %all-reduce = (f32[512]{0:T(512)S(1)}, f32[512]{0:T(512)S(1)}) all-reduce(f32[512]{0:T(512)S(1)} %get-tuple-element.75, f32[512]{0:T(512)S(1)} %get-tuple-element.74), channel_id=1, replica_groups=mesh['grp'=2,'fs'=4,'tp'=4] {'tp'}, use_global_device_ids=true, to_apply=%region_14.15 | all-reduce | flops 1024 | bytes 8192 | tf_op jit(solution)/shard_map/psum | solution.py:62
  (148 shorter events, 63.5 us)
Async XLA Ops:
  6.5 27.7 %copy-start = (bf16[2048,32]{0,1:T(8,128)(2,1)S(1)}, bf16[2048,32]{0,1:T(8,128)(2,1)}, u32[]{:S(2)}) copy-start(bf16[2048,32]{0,1:T(8,128)(2,1)} %param.20) | copy-start | bytes 393220
  6.5 3.4 copy-start.8
  6.5 27.7 %copy-start.9 = (f32[512,256]{1,0:T(8,128)S(1)}, f32[512,256]{1,0:T(8,128)}, u32[]{:S(2)}) copy-start(f32[512,256]{1,0:T(8,128)} %param.23) | copy-start | bytes 1572868
  6.5 27.7 %all-gather.8.cloned.1.call-start = ((), (), s32[]{:S(2)}) async-start(), calls=%async_computation.2 | async-start | bytes 2621440 | tf_op jit(solution)/shard_map/all_gather | solution.py:87
  7.3 56.5 %all-gather.14.cloned.1.call-start = ((), (), s32[]{:S(2)}) async-start(), calls=%async_computation.5 | async-start | bytes 1310720 | tf_op jit(solution)/shard_map/all_gather | solution.py:93
  8.0 84.8 %all-gather.10.cloned.1.call-start = ((), (), s32[]{:S(2)}) async-start(), calls=%async_computation.3 | async-start | bytes 1310720 | tf_op jit(solution)/shard_map/all_gather | solution.py:94
  8.7 130.5 %all-gather.12.cloned.1.call-start = ((), (), s32[]{:S(2)}) async-start(), calls=%async_computation.4 | async-start | bytes 2621440 | tf_op jit(solution)/shard_map/all_gather | solution.py:95
  9.3 176.8 %all-gather.16.cloned.1.call-start = ((), (), s32[]{:S(2)}) async-start(), calls=%async_computation.6 | async-start | bytes 2621440 | tf_op jit(solution)/shard_map/all_gather | solution.py:139
  9.9 210.5 %reduce-scatter.3.cloned.1.call-start = ((), (), s32[]{:S(2)}) async-start(), calls=%async_computation.7 | async-start | bytes 2621440 | tf_op jit(solution)/shard_map/reduce_scatter | solution.py:142
  143.4 1.0 copy-start.4
  143.4 1.2 copy-start.5
  190.3 30.1 %copy-start.2 = (bf16[512,512]{1,0:T(8,128)(2,1)S(1)}, bf16[512,512]{1,0:T(8,128)(2,1)}, u32[]{:S(2)}) copy-start(bf16[512,512]{1,0:T(8,128)(2,1)} %param.16) | copy-start | bytes 1572868
  190.3 37.3 %copy-start.6 = (f32[512]{0:T(512)S(1)}, f32[512]{0:T(512)}, u32[]{:S(2)}) copy-start(f32[512]{0:T(512)} %param.26) | copy-start | bytes 6148
  190.3 284.8 %all-gather.18.cloned.1.call-start = ((), (), s32[]{:S(2)}) async-start(), calls=%async_computation.8 | async-start | bytes 2621440 | tf_op jit(solution)/shard_map/all_gather | solution.py:146
  227.6 3.1 copy-start.3
  229.9 275.1 %all-gather.20.cloned.1.call-start = ((), (), s32[]{:S(2)}) async-start(), calls=%async_computation.9 | async-start | bytes 10485760 | tf_op jit(solution)/shard_map/all_gather | solution.py:150
  230.6 320.3 %reduce-scatter.5.cloned.1.call-start = ((), (), s32[]{:S(2)}) async-start(), calls=%async_computation.10 | async-start | bytes 2621440 | tf_op jit(solution)/shard_map/reduce_scatter | solution.py:157
  230.7 62.7 %collective-permute-start = (bf16[2048,512]{1,0:T(8,128)(2,1)S(1)}, bf16[2048,512]{1,0:T(8,128)(2,1)}, u32[]{:S(2)}, u32[]{:S(2)}) collective-permute-start(bf16[2048,512]{1,0:T(8,128)(2,1)S(1)} %copy-done.3), channel_id=1, source_target_pairs={{0,4},{4,8},{8,12},{12,0},{1,5},{5,9},{9,13},{13,1},{2,6},{6,10},{... | collective-permute-start | bytes 6291464 | tf_op jit(solution)/shard_map/ppermute | solution.py:25
  232.4 213.5 %collective-permute-start.1 = (bf16[2048,512]{1,0:T(8,128)(2,1)S(1)}, bf16[2048,512]{1,0:T(8,128)(2,1)}, u32[]{:S(2)}, u32[]{:S(2)}) collective-permute-start(bf16[2048,512]{1,0:T(8,128)(2,1)S(1)} %copy-done.3), channel_id=1, source_target_pairs={{0,12},{4,0},{8,4},{12,8},{1,13},{5,1},{9,5},{13,9},{2,14},{6,2},{... | collective-permute-start | bytes 6291464 | tf_op jit(solution)/shard_map/ppermute | solution.py:30
  293.4 178.6 %collective-permute-start.2 = (bf16[2048,512]{1,0:T(8,128)(2,1)}, bf16[2048,512]{1,0:T(8,128)(2,1)}, u32[]{:S(2)}, u32[]{:S(2)}) collective-permute-start(bf16[2048,512]{1,0:T(8,128)(2,1)} %collective-permute-done), channel_id=1, source_target_pairs={{0,4},{4,8},{8,12},{12,0},{1,5},{5,9},{9,13},{13,1},{2,6},{6,10},{... | collective-permute-start | bytes 6291464 | tf_op jit(solution)/shard_map/ppermute | solution.py:25
  521.5 29.5 %copy-start.1 = (bf16[512,512]{1,0:T(8,128)(2,1)S(1)}, bf16[512,512]{1,0:T(8,128)(2,1)}, u32[]{:S(2)}) copy-start(bf16[512,512]{1,0:T(8,128)(2,1)} %multiply_convert_fusion.2) | copy-start | bytes 1572868
  521.5 36.6 %copy-start.7 = (f32[512]{0:T(512)S(1)}, f32[512]{0:T(512)}, u32[]{:S(2)}) copy-start(f32[512]{0:T(512)} %param.29) | copy-start | bytes 6148
Sparse Core Ops, SparseCore 0:
  8.9 25.2 all-gather.7
  35.8 27.9 all-gather.13
  65.4 27.3 all-gather.9
  94.2 45.0 all-gather.11
  140.7 44.4 all-gather.15
  190.5 29.9 reduce-scatter.2
  230.0 23.1 all-gather.17
  254.8 250.1 all-gather.19
  521.6 29.2 reduce-scatter.4
